TPU v7x, 256 devices: a whole 4x4x8 slice. The times are simulated.
256 devices in a mesh: sp: 32 (over z, y), tp: 8 (over x, core).
Axes of the slice: x: 4, y: 4, z: 8, core: 2. Of those that a mesh axis runs over, the one named last changes fastest.
Arguments:
- tokens: bfloat16 [4, 16384, 2048], P(None, ('sp', 'tp')), may hold values from -6 to 6
- in_gain: float32 [2048], replicated, may hold values from 0.1 to 1.9
- query_weight: bfloat16 [2048, 1024], P(None, 'tp'), may hold values from -0.125 to 0.125
- key_weight: bfloat16 [2048, 1024], P(None, 'tp'), may hold values from -0.125 to 0.125
- value_weight: bfloat16 [2048, 1024], P(None, 'tp'), may hold values from -0.125 to 0.125
- gate_weight: bfloat16 [2048, 1024], P(None, 'tp'), may hold values from -0.125 to 0.125
- log_decay: float32 [8], P('tp'), may hold values from -0.034 to 0, as said below
- norm_gain: float32 [1024], P('tp'), may hold values from 0.1 to 1.9
- out_weight: bfloat16 [1024, 2048], replicated, may hold values from -0.1875 to 0.1875
- post_gain: float32 [2048], replicated, may hold values from 0.1 to 1.9
Outputs:
- mixed: bfloat16 [4, 16384, 2048], P(None, ('sp', 'tp'))
Inputs may be any that keep to these rules, and one draw needn't show every extreme that they name: `log_decay`: every entry is negative; some heads keep a tenth or more of their memory over 16384 positions, others lose most of it within 30 to 100 positions.
All inputs are finite; a program needn't handle non-finite values.
Results may differ from a plain program's by a relative error of at most 0.015.
Values may be sent and summed in bfloat16 or wider, within the bound.
A program may use at most 64 MiB of HBM per device.

v0:
```python
import jax
import jax.numpy as jnp
from jax import lax
from jax.sharding import Mesh
from jax.sharding import PartitionSpec as P

HEAD_DIM = 128
BLOCK = 128
SP = ("sp_0", "sp_1")
SP_TP = ("sp_0", "sp_1", "tp")
rms_eps = 1e-06
group_eps = 1e-05
rope_base = 10000.0


def neutral_like(shard, identity):
    return jax.tree.map(
        lambda part, zero: jnp.zeros_like(part) + jnp.asarray(zero, part.dtype), shard, identity
    )


def entering(shard, axes, combine, identity):
    before = start = neutral_like(shard, identity)
    running = shard
    for axis in reversed(axes):
        length, mine = (lax.axis_size(axis), lax.axis_index(axis))
        pieces = jax.tree.map(lambda part: lax.all_gather(part, axis), running)
        inside, running = (start, start)
        for k in range(length):
            passed = k < mine
            running = combine(running, jax.tree.map(lambda part: part[k], pieces))
            inside = jax.tree.map(lambda new, old: jnp.where(passed, new, old), running, inside)
        before = combine(inside, before)
    return before


def rotate(values, positions):
    half_dim = values.shape[-1] // 2
    inverse = rope_base ** (-jnp.arange(half_dim, dtype=jnp.float32) / half_dim)
    angles = positions.astype(jnp.float32)[:, None] * inverse[None, :]
    cosine = jnp.cos(angles)
    sine_part = jnp.sin(angles)
    first_half = values[..., :half_dim].astype(jnp.float32)
    second = values[..., half_dim:].astype(jnp.float32)
    return jnp.concatenate(
        [first_half * cosine - second * sine_part, first_half * sine_part + second * cosine],
        axis=-1,
    )


def local_pass(queries, key_rows, values, log_decay):
    seq_count, head_count, length, head_width = queries.shape
    block_count = length // BLOCK
    offsets = jnp.arange(BLOCK, dtype=jnp.float32)
    distance = offsets[:, None] - offsets[None, :]
    rate_col = log_decay[:, None, None]
    inside = jnp.where(distance >= 0, jnp.exp(rate_col * jnp.maximum(distance, 0.0)), 0.0)
    query_scale = jnp.exp(log_decay[:, None] * (offsets + 1.0))[..., None]
    key_scale = jnp.exp(log_decay[:, None] * (BLOCK - 1.0 - offsets))[..., None]
    block_decay = jnp.exp(log_decay * BLOCK)[:, None, None]

    def to_blocks(arr):
        return arr.reshape(seq_count, head_count, block_count, BLOCK, arr.shape[-1]).transpose(
            2, 0, 1, 3, 4
        )

    def advance(memory, inputs):
        q_block, k_block, v_block = inputs
        scores = jnp.einsum("shqd,shkd->shqk", q_block, k_block, preferred_element_type=jnp.float32)
        weights = (scores * inside).astype(jnp.bfloat16)
        within = jnp.einsum("shqk,shkv->shqv", weights, v_block, preferred_element_type=jnp.float32)
        carried = jnp.einsum("shqd,shdv->shqv", q_block.astype(jnp.float32) * query_scale, memory)
        k_scaled = (k_block.astype(jnp.float32) * key_scale).astype(jnp.bfloat16)
        memory = memory * block_decay + jnp.einsum(
            "shkd,shkv->shdv", k_scaled, v_block, preferred_element_type=jnp.float32
        )
        return (memory, within + carried)

    start_memory = jnp.zeros((seq_count, head_count, head_width, values.shape[-1]), jnp.float32)
    end_state, outputs = lax.scan(
        advance, start_memory, (to_blocks(queries), to_blocks(key_rows), to_blocks(values))
    )
    outputs = outputs.transpose(1, 2, 0, 3, 4).reshape(
        seq_count, head_count, length, values.shape[-1]
    )
    return (outputs, end_state)


def combine(earlier, later_part):
    return (
        earlier[0] * later_part[0],
        earlier[1] * later_part[0][None, :, None, None] + later_part[1],
    )


def read_out(carried, queries, partial_out, log_decay):
    length = queries.shape[2]
    read_scale = jnp.exp(log_decay[:, None] * (jnp.arange(length, dtype=jnp.float32) + 1.0))[
        ..., None
    ]
    return partial_out + jnp.einsum(
        "shld,shdv->shlv", queries.astype(jnp.float32) * read_scale, carried
    )


def body(
    tokens,
    in_gain,
    query_weight,
    key_weight,
    value_weight,
    gate_weight,
    log_decay,
    norm_gain,
    out_weight,
    post_gain,
):
    seq_count, rows_dev, model_width = tokens.shape
    tp_size = lax.axis_size("tp")
    local_width = query_weight.shape[1]
    head_count = local_width // HEAD_DIM
    stretch = rows_dev * tp_size
    tok_f32 = tokens.astype(jnp.float32)
    normed = (
        tok_f32 * lax.rsqrt(jnp.mean(tok_f32 * tok_f32, axis=-1, keepdims=True) + rms_eps) * in_gain
    ).astype(jnp.bfloat16)
    joined = jnp.concatenate([query_weight, key_weight, value_weight, gate_weight], axis=1)
    projected = jnp.einsum(
        "kux,xt->kut",
        lax.all_gather(normed, "tp", axis=1, tiled=True),
        joined,
        preferred_element_type=jnp.float32,
    ).astype(jnp.bfloat16)

    def heads_of(columns):
        return columns.reshape(seq_count, stretch, head_count, HEAD_DIM).transpose(0, 2, 1, 3)

    positions = lax.axis_index(SP) * stretch + jnp.arange(stretch, dtype=jnp.int32)
    queries = rotate(heads_of(projected[..., :local_width]), positions).astype(jnp.bfloat16)
    key_rows = (
        rotate(heads_of(projected[..., local_width : 2 * local_width]), positions)
        * HEAD_DIM ** (-0.5)
    ).astype(jnp.bfloat16)
    values = heads_of(projected[..., 2 * local_width : 3 * local_width])
    gating = projected[..., 3 * local_width :]
    partial_out, end_state = local_pass(queries, key_rows, values, log_decay)
    span_decay = jnp.exp(log_decay * stretch)
    carried = entering(
        (span_decay, end_state), SP, combine, (jnp.ones_like(span_decay), jnp.zeros_like(end_state))
    )[1]
    retained = read_out(carried, queries, partial_out, log_decay)
    center = jnp.mean(retained, axis=-1, keepdims=True)
    spread = jnp.mean(jnp.square(retained - center), axis=-1, keepdims=True)
    normal = (
        ((retained - center) * lax.rsqrt(spread + group_eps))
        .transpose(0, 2, 1, 3)
        .reshape(seq_count, stretch, local_width)
    )
    gated = (normal * norm_gain * jax.nn.silu(gating.astype(jnp.float32))).astype(jnp.bfloat16)
    premix = jnp.einsum(
        "hor,rn->hon",
        lax.all_to_all(gated, "tp", split_axis=1, concat_axis=2, tiled=True),
        out_weight,
        preferred_element_type=jnp.float32,
    )
    mixed = (
        premix * lax.rsqrt(jnp.mean(premix * premix, axis=-1, keepdims=True) + rms_eps) * post_gain
    )
    return mixed.astype(jnp.bfloat16)


def solution(mesh):
    torus = Mesh(mesh.devices.reshape(8, 4, mesh.shape["tp"]), ("sp_0", "sp_1", "tp"))
    return jax.shard_map(
        body,
        mesh=torus,
        in_specs=(
            P(None, SP_TP, None),
            P(),
            P(None, "tp"),
            P(None, "tp"),
            P(None, "tp"),
            P(None, "tp"),
            P("tp"),
            P("tp"),
            P(),
            P(),
        ),
        out_specs=P(None, SP_TP, None),
        check_vma=False,
    )
```

profile of v0, /device:TPU:1, one launch (start us, length us, event | category | flops | bytes accessed | tf_op | source)
XLA Modules:
  0.0 204.7 jit_solution(9332395953188734523)
XLA Ops:
  6.5 1.6 fusion.44
  8.1 2.6 %fusion.46 = bf16[4,64,2048]{2,1,0:T(8,128)(2,1)} fusion(bf16[4,64,2048]{2,1,0:T(8,128)(2,1)} %param.12, f32[2048]{0:T(1024)} %param.13, f32[4,64]{1,0:T(4,128)S(1)} %add_rsqrt_fusion.2), kind=kLoop, calls=%fused_computation.48 | loop fusion | flops 2097152 | bytes 2106368 | tf_op jit(solution)/shard_map/convert_element_type | solution.py:126
  11.3 0.5 copy-done.10
  13.0 0.5 multiply_cosine_fusion
  13.5 53.8 %all-gather.7.cloned.1.call-done = bf16[4,512,2048]{2,1,0:T(8,128)(2,1)} async-done(((bf16[4,64,2048]{2,1,0:T(8,128)(2,1)}), bf16[4,512,2048]{2,1,0:T(8,128)(2,1)}) %all-gather.7.cloned.1.call-update) | async-done | bytes 8388624 | tf_op jit(solution)/shard_map/all_gather | solution.py:130
  67.3 9.5 %fusion.54 = bf16[4,512,512]{1,2,0:T(8,128)(2,1)S(1)} fusion(bf16[4,512,2048]{2,1,0:T(8,128)(2,1)} %all-gather.7.cloned.1.call-done, bf16[2048,128]{0,1:T(8,128)(2,1)S(1)} %copy.42, bf16[2048,128]{0,1:T(8,128)(2,1)S(1)} %copy.41, bf16[2048,128]{0,1:T(8,128)(2,1)S(1)} %copy.40, bf16[2048,128]{0,1:T(8,128)(2,1)S(1)} %copy.39), kind=kOutput, calls=%fused_computation.59 | convolution fusion | flops 4304404480 | bytes 12582912 | tf_op jit(solution)/shard_map/kux,xt->kut/dot_general | solution.py:128
  76.9 1.0 slice_bitcast_fusion
  79.8 0.3 copy.43
  80.3 1.3 copy.44
  81.6 1.2 reshape_transpose_reshape.3
  82.8 0.4 copy.45
  83.5 0.9 copy-done.1
  84.4 0.3 fusion.69
  84.8 11.9 %while.15 = (s32[]{:T(128)}, f32[4,1,128,128]{3,2,0,1:T(8,128)S(1)}, f32[4,4,1,128,128]{4,3,1,2,0:T(8,128)}, f32[1]{0:T(128)}, bf16[4,4,1,128,128]{4,3,1,2,0:T(8...) while((s32[]{:T(128)}, ...), condition=%wide.region_2.3_spmd.clone.clone.clone, body=%wide.region_1.2_spmd.clone.clone.clone.sunk | while | flops 67977728 | bytes 2496632 | solution.py:80
  84.8 0.7 select_bitcast_fusion.2
  85.5 0.3 fusion.146
  85.9 0.7 exponential_bitcast_fusion.3
  86.5 0.9 fusion.147
  87.8 0.7 select_bitcast_fusion.2
  88.5 0.3 fusion.146
  88.8 0.7 exponential_bitcast_fusion.3
  89.5 0.9 fusion.147
  90.8 0.7 select_bitcast_fusion.2
  91.8 0.7 exponential_bitcast_fusion.3
  92.5 0.9 fusion.147
  93.8 0.7 select_bitcast_fusion.2
  94.8 0.7 exponential_bitcast_fusion.3
  95.5 0.9 fusion.147
  96.8 0.7 copy-done
  97.5 0.6 dynamic-slice
  98.1 0.7 exponential_dynamic-update-slice_fusion
  98.8 8.4 %all-reduce = f32[4]{0:T(128)S(1)} all-reduce(f32[4]{0:T(128)S(1)} %exponential_dynamic-update-slice_fusion), channel_id=2, replica_groups=mesh['sp_0'=8,'sp_1'=4,'tp'=8] {'sp_1'}, use_global_device_ids=true, to_apply=%add | all-reduce | flops 4 | bytes 32
  107.2 0.7 slice_multiply_fusion.1
  107.9 1.3 slice_multiply_fusion
  109.9 12.2 %all-gather.11.cloned.1.call-done = f32[16,1,128,128]{3,2,1,0:T(8,128)} async-done(((f32[4,1,128,128]{3,2,1,0:T(8,128)}), f32[16,1,128,128]{3,2,1,0:T(8,128)}) %all-gather.11.cloned.1.call-update) | async-done | bytes 1048592 | tf_op jit(solution)/shard_map/all_gather | solution.py:27
  122.0 3.8 %slice_add_fusion.8 = f32[4,1,128,128]{3,2,1,0:T(8,128)} fusion(f32[16,1,128,128]{3,2,1,0:T(8,128)} %all-gather.11.cloned.1.call-done, f32[]{:T(128)} %bitcast.20, f32[]{:T(128)} %bitcast.18, f32[16,1,128,128]{3,2,0,1:T(8,128)} %bitcast.197, f32[]{:T(128)} %bitcast.16, f32[]{:T(128)} %bitcast.13), kind=kLoop, calls=%fused_computation.109 | loop fusion | flops 458752 | bytes 1310736 | tf_op jit(solution)/shard_map/add | solution.py:92
  125.9 0.6 dynamic-slice.1
  126.4 1.3 dynamic-update-slice.1
  127.7 13.9 %all-reduce.1 = f32[8]{0:T(128)S(1)} all-reduce(f32[8]{0:T(128)S(1)} %dynamic-update-slice.1), channel_id=3, replica_groups=mesh['sp_0'=8,'sp_1'=4,'tp'=8] {'sp_0'}, use_global_device_ids=true, to_apply=%add.1 | all-reduce | flops 8 | bytes 64
  141.6 0.7 fusion.127
  145.5 0.4 copy.48
  145.9 0.4 reshape.499
  146.3 18.7 %all-gather.9.cloned.1.call-done = f32[8,4,1,128,128]{4,3,2,1,0:T(8,128)} async-done(((f32[1,4,1,128,128]{4,3,2,1,0:T(8,128)}), f32[8,4,1,128,128]{4,3,2,1,0:T(8,128)}) %all-gather.9.cloned.1.call-update) | async-done | bytes 2097168 | tf_op jit(solution)/shard_map/all_gather | solution.py:27
  165.1 7.9 %fusion.128 = (f32[4,512]{1,0:T(4,128)S(1)}, f32[4,512,128]{1,2,0:T(8,128)S(1)}) fusion(f32[4,512,128]{1,2,0:T(8,128)S(1)} %reshape.499, f32[8,4,1,128,128]{4,3,1,2,0:T(8,128)} %bitcast.204, f32[4,1,128,128]{3,2,1,0:T(8,128)S(1)} %copy-done.4, f32[16,1,128,128]{3,2,0,1:T(8,128)S(1)} %bitcast.198, f32[16,1,128,128]{3,2,1,0:T(8,128)S(1)} %copy-done.3, ...), kind=kOutput, calls=%fused_computation.175 | convolution fusion | flops 71170048 | bytes 5777468 | tf_op jit(solution)/shard_map/shld,shdv->shlv/dot_general | solution.py:101
  173.2 1.5 fusion.62
  175.0 18.3 %all_to_all.18 = bf16[4,512,128]{2,0,1:T(4,128)(2,1)S(1)} all-to-all(bf16[4,512,128]{2,0,1:T(4,128)(2,1)S(1)} %copy.65), channel_id=1, replica_groups=mesh['sp_0'=8,'sp_1'=4,'tp'=8] {'tp'}, dimensions={1} | all-to-all | bytes 1048576 | tf_op jit(solution)/shard_map/all_to_all | solution.py:162
  193.4 3.6 %multiply_reduce_fusion = (f32[4,64]{1,0:T(4,128)S(1)}, f32[4,64,2048]{2,1,0:T(8,128)S(1)}) fusion(bf16[1024,2048]{1,0:T(8,128)(2,1)} %param.20, bf16[4,8,8,8,128]{4,3,2,1,0:T(8,128)(2,1)S(1)} %bitcast.203), kind=kOutput, calls=%fused_computation.58 | convolution fusion | flops 1074790144 | bytes 6816768 | tf_op jit(solution)/shard_map/hor,rn->hon/dot_general | solution.py:160
  197.0 1.2 multiply_convert_fusion.2
  (67 shorter events, 5.9 us)
Async XLA Ops:
  6.5 4.3 %copy-start.8 = (bf16[2048,128]{1,0:T(8,128)(2,1)S(1)}, bf16[2048,128]{1,0:T(8,128)(2,1)}, u32[]{:S(2)}) copy-start(bf16[2048,128]{1,0:T(8,128)(2,1)} %param.14) | copy-start | bytes 1572868
  6.5 60.8 %all-gather.7.cloned.1.call-start = ((), (), s32[]{:S(2)}) async-start(), calls=%async_computation.1 | async-start | bytes 9437184 | tf_op jit(solution)/shard_map/all_gather | solution.py:130
  8.1 3.0 %copy-start.9 = (bf16[2048,128]{1,0:T(8,128)(2,1)S(1)}, bf16[2048,128]{1,0:T(8,128)(2,1)}, u32[]{:S(2)}) copy-start(bf16[2048,128]{1,0:T(8,128)(2,1)} %param.15) | copy-start | bytes 1572868
  10.8 1.0 copy-start.10
  10.8 1.3 copy-start.11
  10.8 111.2 %all-gather.11.cloned.1.call-start = ((), (), s32[]{:S(2)}) async-start(), calls=%async_computation.3 | async-start | bytes 1310720 | tf_op jit(solution)/shard_map/all_gather | solution.py:27
  76.9 1.5 copy-start.2
  78.3 0.7 copy-start.6
  78.4 0.8 copy-start.7
  83.2 1.2 copy-start.1
  84.8 12.8 %copy-start.15 = (u32[256]{0:T(256)S(1)}, u32[256]{0:T(256)}, u32[]{:S(2)}) copy-start(u32[256]{0:T(256)} %constant.86) | copy-start | bytes 3076
  84.8 41.1 %copy-start.14 = (u32[256]{0:T(256)S(1)}, u32[256]{0:T(256)}, u32[]{:S(2)}) copy-start(u32[256]{0:T(256)} %constant.91) | copy-start | bytes 3076
  96.7 0.7 copy-start
  96.7 48.7 %copy-start.5 = (f32[4,4,1,128,128]{4,3,1,2,0:T(8,128)S(1)}, f32[4,4,1,128,128]{4,3,1,2,0:T(8,128)}, u32[]{:S(2)}) copy-start(f32[4,4,1,128,128]{4,3,1,2,0:T(8,128)} %get-tuple-element.58) | copy-start | bytes 3145732
  97.5 67.6 %all-gather.9.cloned.1.call-start = ((), (), s32[]{:S(2)}) async-start(), calls=%async_computation.2 | async-start | bytes 2359296 | tf_op jit(solution)/shard_map/all_gather | solution.py:27
  145.5 19.6 %copy-start.3 = (f32[16,1,128,128]{3,2,1,0:T(8,128)S(1)}, f32[16,1,128,128]{3,2,1,0:T(8,128)}, u32[]{:S(2)}) copy-start(f32[16,1,128,128]{3,2,1,0:T(8,128)} %all-gather.11.cloned.1.call-done) | copy-start | bytes 3145732
  145.5 19.6 %copy-start.4 = (f32[4,1,128,128]{3,2,1,0:T(8,128)S(1)}, f32[4,1,128,128]{3,2,1,0:T(8,128)}, u32[]{:S(2)}) copy-start(f32[4,1,128,128]{3,2,1,0:T(8,128)} %slice_add_fusion.8) | copy-start | bytes 786436
  165.1 8.1 %copy-start.13 = (f32[128]{0:T(128)S(1)}, f32[128]{0:T(128)}, u32[]{:S(2)}) copy-start(f32[128]{0:T(128)} %param.19) | copy-start | bytes 1540
  193.4 3.6 %copy-start.12 = (f32[2048]{0:T(1024)S(1)}, f32[2048]{0:T(1024)}, u32[]{:S(2)}) copy-start(f32[2048]{0:T(1024)} %param.21) | copy-start | bytes 24580
Sparse Core Ops, SparseCore 0:
  10.9 56.3 all-gather.6
  97.6 24.3 all-gather.10
  126.0 39.0 all-gather.8
where the time goes:
time: 205 us
  waiting for transfers between devices  84.8 us (41%)
  blocking collectives  40.6 us (20%)
  matrix products  27.4 us (13%)
  other arithmetic  20.4 us (10%)
  between operations  18 us (9%)
  local copies, waits for them, and re-layouts  13.3 us (6%)
    all_gather x1, waiting for transfers between devices, body(): lax.all_gather(normed, 'tp', axis=1, tiled=True)  53.8 us
    all_gather x2, waiting for transfers between devices, entering(): pieces = jax.tree.map(lambda part: lax.all_gather(part, axis), running)  30.9 us
    unnamed x2, blocking collectives  22.3 us
    all_to_all x1, blocking collectives, body(): lax.all_to_all(gated, 'tp', split_axis=1, concat_axis=2, tiled=True)  18.3 us
    dot_general x1, matrix products, body(): jnp.einsum('kux,xt->kut', lax.all_gather(normed, 'tp', axis=1, tiled=True...  9.51 us
    dot_general x1, matrix products, read_out(): jnp.einsum('shld,shdv->shlv', queries.astype(jnp.float32) * read_scale, c...  7.93 us
    unnamed x41, local copies, waits for them, and re-layouts  6.03 us
  transfers between devices with their start and end apart: 3, of which 3 were waited for; matrix products, arithmetic and copies ran while one was open for 4% of the time, Pallas kernels for 0%

commit v1 on v0

--- a/solution.py
+++ b/solution.py
@@ -11,6 +11,11 @@
 rms_eps = 1e-06
 group_eps = 1e-05
 rope_base = 10000.0
+
+
+def exchange_gather(shard, mesh_axis, dim):
+    repeated = jnp.stack([shard] * lax.axis_size(mesh_axis))
+    return jnp.concatenate(lax.all_to_all(repeated, mesh_axis, 0, 0), axis=dim)
 
 
 def neutral_like(shard, identity):
@@ -126,10 +131,7 @@
     ).astype(jnp.bfloat16)
     joined = jnp.concatenate([query_weight, key_weight, value_weight, gate_weight], axis=1)
     projected = jnp.einsum(
-        "kux,xt->kut",
-        lax.all_gather(normed, "tp", axis=1, tiled=True),
-        joined,
-        preferred_element_type=jnp.float32,
+        "kux,xt->kut", exchange_gather(normed, "tp", 1), joined, preferred_element_type=jnp.float32
     ).astype(jnp.bfloat16)
 
     def heads_of(columns):

time: 205 us -> 263 us (1.28)
  waiting for transfers between devices: 84.8 us -> 123 us
  local copies, waits for them, and re-layouts: 13.3 us -> 26.1 us
  starting transfers between devices: 0.09 us -> 8.23 us
    all_to_all x0 -> x1, waiting for transfers between devices: none -> 91 us  [exchange_gather(): return jnp.concatenate(lax.all_to_all(repeated, mesh_axis, 0, 0), axis=dim)]
    all_gather x1 -> x0, waiting for transfers between devices: 53.8 us -> none  [body(): lax.all_gather(normed, 'tp', axis=1, tiled=True)]
    reshape x0 -> x1, local copies, waits for them, and re-layouts: none -> 8.28 us  [exchange_gather(): return jnp.concatenate(lax.all_to_all(repeated, mesh_axis, 0, 0), axis=dim)]
    all_to_all x0 -> x1, starting transfers between devices: none -> 8.15 us  [exchange_gather(): return jnp.concatenate(lax.all_to_all(repeated, mesh_axis, 0, 0), axis=dim)]
    another operation x0 -> x1, local copies, waits for them, and re-layouts: none -> 4.3 us  [exchange_gather(): repeated = jnp.stack([shard] * lax.axis_size(mesh_axis))]
  transfers between devices with their start and end apart: 3 -> 3, of which waited for: 3 -> 3; matrix products, arithmetic and copies ran while one was open for 4% -> 3% of each run, Pallas kernels for 0% -> 0%
where the time goes in v1:
time: 263 us; the launch traced here: 262 us
  waiting for transfers between devices  123 us (47%)
  blocking collectives  39.5 us (15%)
  matrix products  27.4 us (10%)
  local copies, waits for them, and re-layouts  26.1 us (10%)
  other arithmetic  19.3 us (7%)
  between operations  18.3 us (7%)
  starting transfers between devices  8.23 us (3%)
    all_to_all x1, waiting for transfers between devices, exchange_gather(): return jnp.concatenate(lax.all_to_all(repeated, mesh_axis, 0, 0), axis=dim)  91 us
    all_gather x2, waiting for transfers between devices, entering(): pieces = jax.tree.map(lambda part: lax.all_gather(part, axis), running)  31.9 us
    unnamed x2, blocking collectives  20.9 us
    all_to_all x1, blocking collectives, body(): lax.all_to_all(gated, 'tp', split_axis=1, concat_axis=2, tiled=True)  18.7 us
    dot_general x1, matrix products, body(): jnp.einsum('kux,xt->kut', exchange_gather(normed, 'tp', 1), joined, prefe...  9.51 us
    reshape x1, local copies, waits for them, and re-layouts, exchange_gather(): return jnp.concatenate(lax.all_to_all(repeated, mesh_axis, 0, 0), axis=dim)  8.28 us
    all_to_all x1, starting transfers between devices, exchange_gather(): return jnp.concatenate(lax.all_to_all(repeated, mesh_axis, 0, 0), axis=dim)  8.15 us
    dot_general x1, matrix products, read_out(): jnp.einsum('shld,shdv->shlv', queries.astype(jnp.float32) * read_scale, c...  7.98 us
  transfers between devices with their start and end apart: 3, of which 3 were waited for; matrix products, arithmetic and copies ran while one was open for 3% of the time, Pallas kernels for 0%

profile of v1, /device:TPU:1, one launch (start us, length us, event | category | flops | bytes accessed | tf_op | source)
XLA Modules:
  0.0 262.0 jit_solution(14239087087213979959)
XLA Ops:
  6.5 1.5 fusion.44
  8.1 1.5 fusion.46
  9.6 4.3 %stack.2 = bf16[8,4,64,2048]{3,2,1,0:T(8,128)(2,1)} broadcast(bf16[4,64,2048]{2,1,0:T(8,128)(2,1)S(1)} %fusion.46), dimensions={1,2,3} | broadcast | bytes 9437184 | tf_op jit(solution)/shard_map/stack | solution.py:17
  13.9 8.2 %all-to-all-start = ((bf16[8,4,64,2048]{3,2,1,0:T(8,128)(2,1)}), bf16[8,4,64,2048]{3,2,1,0:T(8,128)(2,1)}, u32[]{:S(2)}, u32[]{:S(2)}) async-start(bf16[8,4,64,2048]{3,2,1,0:T(8,128)(2,1)} %stack.2), calls=%async_computation | async-start | bytes 16777216 | tf_op jit(solution)/shard_map/all_to_all | solution.py:18
  22.6 0.5 copy-done.10
  24.3 0.5 multiply_cosine_fusion
  24.8 91.0 %all-to-all-done = bf16[8,4,64,2048]{3,2,1,0:T(8,128)(2,1)} async-done(((bf16[8,4,64,2048]{3,2,1,0:T(8,128)(2,1)}), bf16[8,4,64,2048]{3,2,1,0:T(8,128)(2,1)}, u32[]{:S(2)}, u32[]{:S(2)}) %all-to-all-start) | async-done | bytes 8388640 | tf_op jit(solution)/shard_map/all_to_all | solution.py:18
  115.8 8.3 %copy.39 = bf16[4,8,64,2048]{3,2,1,0:T(8,128)(2,1)} copy(bf16[4,8,64,2048]{3,2,0,1:T(8,128)(2,1)} %bitcast) | data formatting | bytes 16777216 | tf_op jit(solution)/shard_map/reshape | solution.py:18
  124.1 9.5 %fusion.54 = bf16[4,512,512]{1,2,0:T(8,128)(2,1)S(1)} fusion(bf16[4,512,2048]{2,1,0:T(8,128)(2,1)} %bitcast.198, bf16[2048,128]{0,1:T(8,128)(2,1)S(1)} %copy.43, bf16[2048,128]{0,1:T(8,128)(2,1)S(1)} %copy.42, bf16[2048,128]{0,1:T(8,128)(2,1)S(1)} %copy.41, bf16[2048,128]{0,1:T(8,128)(2,1)S(1)} %copy.40), kind=kOutput, calls=%fused_computation.59 | convolution fusion | flops 4304404480 | bytes 12582912 | tf_op jit(solution)/shard_map/kux,xt->kut/dot_general | solution.py:133
  133.6 1.0 slice_bitcast_fusion
  136.5 0.3 copy.44
  137.1 1.3 copy.45
  138.4 1.2 reshape_transpose_reshape.3
  139.6 0.4 copy.46
  140.3 0.9 copy-done.1
  141.6 11.9 %while.15 = (s32[]{:T(128)}, f32[4,1,128,128]{3,2,0,1:T(8,128)S(1)}, f32[4,4,1,128,128]{4,3,1,2,0:T(8,128)}, f32[1]{0:T(128)}, bf16[4,4,1,128,128]{4,3,1,2,0:T(8...) while((s32[]{:T(128)}, ...), condition=%wide.region_2.3_spmd.clone.clone.clone, body=%wide.region_1.2_spmd.clone.clone.clone.sunk | while | flops 67977728 | bytes 2496632 | solution.py:85
  141.6 0.7 select_bitcast_fusion.2
  142.6 0.7 exponential_bitcast_fusion.3
  143.3 0.9 fusion.147
  144.5 0.7 select_bitcast_fusion.2
  145.6 0.7 exponential_bitcast_fusion.3
  146.2 0.9 fusion.147
  147.5 0.7 select_bitcast_fusion.2
  148.6 0.7 exponential_bitcast_fusion.3
  149.2 0.9 fusion.147
  150.5 0.7 select_bitcast_fusion.2
  151.5 0.7 exponential_bitcast_fusion.3
  152.2 0.9 fusion.147
  153.5 0.7 copy-done
  154.3 0.7 dynamic-slice
  154.9 0.7 exponential_dynamic-update-slice_fusion
  155.7 7.0 %all-reduce = f32[4]{0:T(128)S(1)} all-reduce(f32[4]{0:T(128)S(1)} %exponential_dynamic-update-slice_fusion), channel_id=2, replica_groups=mesh['sp_0'=8,'sp_1'=4,'tp'=8] {'sp_1'}, use_global_device_ids=true, to_apply=%add | all-reduce | flops 4 | bytes 32
  162.7 0.7 slice_multiply_fusion.1
  163.3 1.2 slice_multiply_fusion
  165.2 13.5 %all-gather.8.cloned.1.call-done = f32[16,1,128,128]{3,2,1,0:T(8,128)} async-done(((f32[4,1,128,128]{3,2,1,0:T(8,128)}), f32[16,1,128,128]{3,2,1,0:T(8,128)}) %all-gather.8.cloned.1.call-update) | async-done | bytes 1048592 | tf_op jit(solution)/shard_map/all_gather | solution.py:32
  178.7 3.9 %slice_add_fusion.8 = f32[4,1,128,128]{3,2,1,0:T(8,128)} fusion(f32[16,1,128,128]{3,2,1,0:T(8,128)} %all-gather.8.cloned.1.call-done, f32[]{:T(128)} %bitcast.22, f32[]{:T(128)} %bitcast.20, f32[16,1,128,128]{3,2,0,1:T(8,128)} %bitcast.200, f32[]{:T(128)} %bitcast.18, f32[]{:T(128)} %bitcast.15), kind=kLoop, calls=%fused_computation.109 | loop fusion | flops 458752 | bytes 1310736 | tf_op jit(solution)/shard_map/add | solution.py:97
  182.6 0.6 dynamic-slice.1
  183.2 1.4 dynamic-update-slice.1
  184.5 13.9 %all-reduce.1 = f32[8]{0:T(128)S(1)} all-reduce(f32[8]{0:T(128)S(1)} %dynamic-update-slice.1), channel_id=3, replica_groups=mesh['sp_0'=8,'sp_1'=4,'tp'=8] {'sp_0'}, use_global_device_ids=true, to_apply=%add.1 | all-reduce | flops 8 | bytes 64
  198.4 0.7 fusion.127
  202.3 0.4 copy.49
  202.7 0.4 reshape.509
  203.1 18.4 %all-gather.6.cloned.1.call-done = f32[8,4,1,128,128]{4,3,2,1,0:T(8,128)} async-done(((f32[1,4,1,128,128]{4,3,2,1,0:T(8,128)}), f32[8,4,1,128,128]{4,3,2,1,0:T(8,128)}) %all-gather.6.cloned.1.call-update) | async-done | bytes 2097168 | tf_op jit(solution)/shard_map/all_gather | solution.py:32
  221.6 8.0 %fusion.128 = (f32[4,512]{1,0:T(4,128)S(1)}, f32[4,512,128]{1,2,0:T(8,128)S(1)}) fusion(f32[4,512,128]{1,2,0:T(8,128)S(1)} %reshape.509, f32[8,4,1,128,128]{4,3,1,2,0:T(8,128)} %bitcast.207, f32[4,1,128,128]{3,2,1,0:T(8,128)S(1)} %copy-done.4, f32[16,1,128,128]{3,2,0,1:T(8,128)S(1)} %bitcast.201, f32[16,1,128,128]{3,2,1,0:T(8,128)S(1)} %copy-done.3, ...), kind=kOutput, calls=%fused_computation.175 | convolution fusion | flops 71170048 | bytes 5777468 | tf_op jit(solution)/shard_map/shld,shdv->shlv/dot_general | solution.py:106
  229.8 1.5 fusion.62
  231.5 18.7 %all_to_all.23 = bf16[4,512,128]{2,0,1:T(4,128)(2,1)S(1)} all-to-all(bf16[4,512,128]{2,0,1:T(4,128)(2,1)S(1)} %copy.66), channel_id=1, replica_groups=mesh['sp_0'=8,'sp_1'=4,'tp'=8] {'tp'}, dimensions={1} | all-to-all | bytes 1048576 | tf_op jit(solution)/shard_map/all_to_all | solution.py:164
  250.3 3.6 %multiply_reduce_fusion = (f32[4,64]{1,0:T(4,128)S(1)}, f32[4,64,2048]{2,1,0:T(8,128)S(1)}) fusion(bf16[1024,2048]{1,0:T(8,128)(2,1)} %param.20, bf16[4,8,8,8,128]{4,3,2,1,0:T(8,128)(2,1)S(1)} %bitcast.206), kind=kOutput, calls=%fused_computation.58 | convolution fusion | flops 1074790144 | bytes 6816768 | tf_op jit(solution)/shard_map/hor,rn->hon/dot_general | solution.py:162
  253.9 1.2 multiply_convert_fusion.2
  (68 shorter events, 6.9 us)
Async XLA Ops:
  13.9 8.2 %copy-start.8 = (bf16[2048,128]{1,0:T(8,128)(2,1)S(1)}, bf16[2048,128]{1,0:T(8,128)(2,1)}, u32[]{:S(2)}) copy-start(bf16[2048,128]{1,0:T(8,128)(2,1)} %param.14) | copy-start | bytes 1572868
  13.9 8.5 %copy-start.9 = (bf16[2048,128]{1,0:T(8,128)(2,1)S(1)}, bf16[2048,128]{1,0:T(8,128)(2,1)}, u32[]{:S(2)}) copy-start(bf16[2048,128]{1,0:T(8,128)(2,1)} %param.15) | copy-start | bytes 1572868
  13.9 101.9 %all-to-all-start = ((bf16[8,4,64,2048]{3,2,1,0:T(8,128)(2,1)}), bf16[8,4,64,2048]{3,2,1,0:T(8,128)(2,1)}, u32[]{:S(2)}, u32[]{:S(2)}) async-start(bf16[8,4,64,2048]{3,2,1,0:T(8,128)(2,1)} %stack.2), calls=%async_computation | async-start | bytes 16777216 | tf_op jit(solution)/shard_map/all_to_all | solution.py:18
  22.1 1.0 copy-start.10
  22.1 1.3 copy-start.11
  22.1 156.6 %all-gather.8.cloned.1.call-start = ((), (), s32[]{:S(2)}) async-start(), calls=%async_computation.3 | async-start | bytes 1310720 | tf_op jit(solution)/shard_map/all_gather | solution.py:32
  133.6 1.5 copy-start.2
  135.1 0.7 copy-start.6
  135.1 0.8 copy-start.7
  140.0 1.2 copy-start.1
  141.5 12.8 %copy-start.15 = (u32[256]{0:T(256)S(1)}, u32[256]{0:T(256)}, u32[]{:S(2)}) copy-start(u32[256]{0:T(256)} %constant.86) | copy-start | bytes 3076
  141.5 41.0 %copy-start.14 = (u32[256]{0:T(256)S(1)}, u32[256]{0:T(256)}, u32[]{:S(2)}) copy-start(u32[256]{0:T(256)} %constant.91) | copy-start | bytes 3076
  153.5 0.7 copy-start
  153.5 48.8 %copy-start.5 = (f32[4,4,1,128,128]{4,3,1,2,0:T(8,128)S(1)}, f32[4,4,1,128,128]{4,3,1,2,0:T(8,128)}, u32[]{:S(2)}) copy-start(f32[4,4,1,128,128]{4,3,1,2,0:T(8,128)} %get-tuple-element.58) | copy-start | bytes 3145732
  154.2 67.3 %all-gather.6.cloned.1.call-start = ((), (), s32[]{:S(2)}) async-start(), calls=%async_computation.2 | async-start | bytes 2359296 | tf_op jit(solution)/shard_map/all_gather | solution.py:32
  202.3 19.3 %copy-start.3 = (f32[16,1,128,128]{3,2,1,0:T(8,128)S(1)}, f32[16,1,128,128]{3,2,1,0:T(8,128)}, u32[]{:S(2)}) copy-start(f32[16,1,128,128]{3,2,1,0:T(8,128)} %all-gather.8.cloned.1.call-done) | copy-start | bytes 3145732
  202.3 19.3 %copy-start.4 = (f32[4,1,128,128]{3,2,1,0:T(8,128)S(1)}, f32[4,1,128,128]{3,2,1,0:T(8,128)}, u32[]{:S(2)}) copy-start(f32[4,1,128,128]{3,2,1,0:T(8,128)} %slice_add_fusion.8) | copy-start | bytes 786436
  221.6 8.2 %copy-start.13 = (f32[128]{0:T(128)S(1)}, f32[128]{0:T(128)}, u32[]{:S(2)}) copy-start(f32[128]{0:T(128)} %param.19) | copy-start | bytes 1540
  250.3 3.6 %copy-start.12 = (f32[2048]{0:T(1024)S(1)}, f32[2048]{0:T(1024)}, u32[]{:S(2)}) copy-start(f32[2048]{0:T(1024)} %param.21) | copy-start | bytes 24580
Sparse Core Ops, SparseCore 0:
  154.3 24.2 all-gather.7
  182.7 38.8 all-gather.5
